TPU v7x, 512 devices: a whole 4x8x8 slice. The times are simulated.
512 devices in a mesh: sp: 64 (over z, y), tp: 8 (over x, core).
Axes of the slice: x: 4, y: 8, z: 8, core: 2. Of those that a mesh axis runs over, the one named last changes fastest.
Arguments:
- latent: bfloat16 [16384, 2048], P('sp'), may hold values from -6 to 6
- context: bfloat16 [512, 2048], P('sp'), may hold values from -6 to 6
- cond: bfloat16 [2048], P('sp'), may hold values from -6 to 6
- cond_ctx: bfloat16 [2048], P('sp'), may hold values from -6 to 6
- shift_weight: bfloat16 [2048, 2048], P('sp', 'tp'), may hold values from -0.125 to 0.125
- scale_weight: bfloat16 [2048, 2048], P('sp', 'tp'), may hold values from -0.125 to 0.125
- gate_weight: bfloat16 [2048, 2048], P('sp', 'tp'), may hold values from -0.25 to 0.25
- norm_gain: bfloat16 [2048], replicated, may hold values from 0.099609375 to 1.8984375
- query_weight: bfloat16 [2048, 1024], P(None, 'tp'), may hold values from -0.125 to 0.125
- key_weight: bfloat16 [2048, 1024], P(None, 'tp'), may hold values from -0.125 to 0.125
- value_weight: bfloat16 [2048, 1024], P(None, 'tp'), may hold values from -0.125 to 0.125
- query_gain: bfloat16 [64], replicated, may hold values from 0.099609375 to 1.8984375
- key_gain: bfloat16 [64], replicated, may hold values from 0.099609375 to 1.8984375
- offset_bias: float32 [16, 15, 31], P('tp'), may hold values from -0.5 to 251
- out_weight: bfloat16 [1024, 2048], P(None, 'tp'), may hold values from -1.5 to 1.5
Outputs:
- updated: bfloat16 [16384, 2048], P('sp', 'tp')
All inputs are finite; a program needn't handle non-finite values.
Results may differ from a plain program's by a relative error of at most 0.0077.
Values may be sent and summed in bfloat16 or wider, within the bound.
A program may use at most 64 MiB of HBM per device.

v0:
```python
import jax
import jax.numpy as jnp
import numpy as np
from jax import lax
from jax.sharding import Mesh
from jax.sharding import PartitionSpec as P

HEAD_DIM = 64
WIN_ROWS = 8
WIN_COLS = 16
GRID_W = 64
SP = ("sp_0", "sp_1")


EPS = 1e-06


def one_axis_at_a_time(x, axes):
    for axis in axes:
        x = lax.psum(x, axis)
    return x


def in_order(pieces, dim):
    dims = list(pieces.shape[1:])
    dims[dim] *= pieces.shape[0]
    return jnp.moveaxis(pieces, 0, dim).reshape(dims)


def sent_to_all(x, axis):
    copies = jnp.broadcast_to(x, (lax.axis_size(axis), *x.shape))
    return lax.all_to_all(copies, axis, split_axis=0, concat_axis=0, tiled=True)


def collect(x, axis, dim):
    return in_order(sent_to_all(x, axis), dim)


def side_by_side(arrays, axis, dim, along):
    widths = [a.shape[along] for a in arrays]
    both = jnp.concatenate(arrays, axis=along)
    result = collect(both, axis, dim)
    return tuple(jnp.split(result, [sum(widths[:k]) for k in range(1, len(widths))], axis=along))


def padded_2(block, sides, width):
    for axis, dim in sides:
        count = lax.axis_size(axis)
        forward = [(i, i + 1) for i in range(count - 1)]
        backward = [(target, source) for source, target in forward]
        low = lax.ppermute(
            lax.slice_in_dim(block, block.shape[dim] - width, None, axis=dim), axis, forward
        )
        high = lax.ppermute(lax.slice_in_dim(block, 0, width, axis=dim), axis, backward)
        block = jnp.concatenate([low, block, high], axis=dim)
    return block


def modulate(rows, norm_gain, scale, shift):
    values = rows.astype(jnp.float32)
    normed = values * lax.rsqrt(jnp.mean(values * values, axis=-1, keepdims=True) + EPS)
    return (normed * norm_gain.astype(jnp.float32) * (1.0 + scale) + shift).astype(jnp.bfloat16)


def project_heads(hidden, weight, gain):
    raw = jnp.dot(hidden, weight, preferred_element_type=jnp.float32)
    split = raw.reshape(hidden.shape[0], -1, HEAD_DIM)
    if gain is None:
        return split.astype(jnp.bfloat16)
    normed = split * lax.rsqrt(jnp.mean(split * split, axis=-1, keepdims=True) + EPS)
    return (normed * gain.astype(jnp.float32)).astype(jnp.bfloat16)


def body(
    latent,
    context,
    cond,
    cond_ctx,
    shift_weight,
    scale_weight,
    gate_weight,
    norm_gain,
    query_weight,
    key_weight,
    value_weight,
    query_gain,
    key_gain,
    offset_bias,
    out_weight,
):
    col_width = shift_weight.shape[1]
    tp_offset = lax.axis_index("tp") * col_width
    act = jax.nn.silu(cond.astype(jnp.float32)).astype(jnp.bfloat16)
    act_ctx = jax.nn.silu(cond_ctx.astype(jnp.float32)).astype(jnp.bfloat16)
    acts = jnp.stack([act, act_ctx])
    terms = jnp.concatenate(
        [
            jnp.dot(acts, shift_weight, preferred_element_type=jnp.float32),
            jnp.dot(acts, scale_weight, preferred_element_type=jnp.float32),
            jnp.dot(acts[:1], gate_weight, preferred_element_type=jnp.float32),
        ],
        axis=0,
    )
    summed = one_axis_at_a_time(terms, SP)
    full = collect(summed, "tp", 1)
    shift, shift_ctx, scale, scale_ctx, gate = (full[0], full[1], full[2], full[3], full[4])
    heads_dev = offset_bias.shape[0]
    lane = heads_dev * HEAD_DIM
    hidden_ctx = modulate(context, norm_gain, scale_ctx, shift_ctx)
    own_keys = project_heads(hidden_ctx, key_weight, key_gain).reshape(context.shape[0], lane)
    own_values = project_heads(hidden_ctx, value_weight, None).reshape(context.shape[0], lane)
    ctx_keys, ctx_values = side_by_side((own_keys, own_values), SP, 0, 1)
    ctx_keys = ctx_keys.reshape(-1, heads_dev, HEAD_DIM)
    ctx_values = ctx_values.reshape(-1, heads_dev, HEAD_DIM)
    hidden = modulate(latent, norm_gain, scale, shift)
    queries = project_heads(hidden, query_weight, query_gain)
    keys = project_heads(hidden, key_weight, key_gain)
    values = project_heads(hidden, value_weight, None)
    rows_dev = latent.shape[0] // GRID_W
    reach = WIN_ROWS // 2
    grid_kv = jnp.stack(
        [keys.reshape(rows_dev, GRID_W, lane), values.reshape(rows_dev, GRID_W, lane)], axis=1
    )
    padded = padded_2(grid_kv, ((SP, 0),), reach)
    total_rows = rows_dev * lax.axis_size(SP)
    base = lax.axis_index(SP) * rows_dev
    local_rows = base + jnp.arange(rows_dev, dtype=jnp.int32)
    first = jnp.clip(local_rows - reach, 0, total_rows - WIN_ROWS)
    window_rows = jnp.arange(WIN_ROWS, dtype=jnp.int32)
    band_index = (first - base + reach)[:, None] + window_rows[None, :]
    band = jnp.take(padded, band_index, axis=0)
    n_blocks = GRID_W // WIN_COLS
    span = 2 * WIN_COLS
    starts = [
        min(max(block * WIN_COLS - WIN_COLS // 2, 0), GRID_W - span) for block in range(n_blocks)
    ]
    blocked = jnp.stack([band[:, :, :, begin : begin + span] for begin in starts], axis=3)
    blocked = blocked.reshape(rows_dev, WIN_ROWS, 2, n_blocks, span, heads_dev, HEAD_DIM)
    key_blocks = blocked[:, :, 0]
    value_blocks = blocked[:, :, 1]
    query_col = np.arange(n_blocks)[:, None, None] * WIN_COLS + np.arange(WIN_COLS)[None, :, None]
    key_col = np.array(starts)[:, None, None] + np.arange(span)[None, None, :]
    window_first = np.clip(query_col - WIN_COLS // 2, 0, GRID_W - WIN_COLS)
    inside = (key_col >= window_first) & (key_col < window_first + WIN_COLS)
    col_offset = np.clip(key_col - query_col + WIN_COLS - 1, 0, 2 * WIN_COLS - 2)
    col_onehot = (col_offset[..., None] == np.arange(2 * WIN_COLS - 1)).astype(np.float32)
    row_offset = first[:, None] + window_rows[None, :] - local_rows[:, None] + WIN_ROWS - 1
    row_onehot = (row_offset[..., None] == jnp.arange(2 * WIN_ROWS - 1, dtype=jnp.int32)).astype(
        jnp.float32
    )
    by_col = jnp.einsum(
        "hxc,bqkc->hxbqk", offset_bias, jnp.asarray(col_onehot), precision=lax.Precision.HIGHEST
    )
    bias = jnp.einsum("rjx,hxbqk->rhbqjk", row_onehot, by_col, precision=lax.Precision.HIGHEST)
    factor = HEAD_DIM ** (-0.5)
    grid_q = queries.reshape(rows_dev, n_blocks, WIN_COLS, heads_dev, HEAD_DIM)
    local_scores = (
        jnp.einsum("rbqhd,rjbkhd->rhbqjk", grid_q, key_blocks, preferred_element_type=jnp.float32)
        * factor
    )
    local_scores = jnp.where(jnp.asarray(inside)[:, :, None, :], local_scores + bias, -jnp.inf)
    band_len = WIN_ROWS * span
    local_scores = local_scores.reshape(rows_dev, heads_dev, n_blocks, WIN_COLS, band_len)
    ctx_scores = (
        jnp.einsum("rbqhd,chd->rhbqc", grid_q, ctx_keys, preferred_element_type=jnp.float32)
        * factor
    )
    scores = jnp.concatenate([local_scores, ctx_scores], axis=-1)
    top = jnp.max(scores, axis=-1, keepdims=True)
    expd = jnp.exp(scores - top)
    weights = (expd / jnp.sum(expd, axis=-1, keepdims=True)).astype(jnp.bfloat16)
    local_w = weights[..., :band_len].reshape(
        rows_dev, heads_dev, n_blocks, WIN_COLS, WIN_ROWS, span
    )
    mixed = jnp.einsum(
        "rhbqjk,rjbkhd->rbqhd", local_w, value_blocks, preferred_element_type=jnp.float32
    )
    mixed = mixed + jnp.einsum(
        "rhbqc,chd->rbqhd", weights[..., band_len:], ctx_values, preferred_element_type=jnp.float32
    )
    mixed = mixed.astype(jnp.bfloat16).reshape(latent.shape[0], lane)
    projected = jnp.dot(collect(mixed, "tp", 1), out_weight, preferred_element_type=jnp.float32)
    own_cols = lax.dynamic_slice_in_dim(latent, tp_offset, col_width, 1).astype(jnp.float32)
    gate_cols = lax.dynamic_slice_in_dim(gate, tp_offset, col_width, 0)
    return (own_cols + gate_cols[None, :] * projected).astype(jnp.bfloat16)


def solution(mesh):
    split = Mesh(mesh.devices.reshape(8, 8, mesh.shape["tp"]), ("sp_0", "sp_1", "tp"))
    placed = (
        P(SP, None),
        P(SP, None),
        P(SP),
        P(SP),
        P(SP, "tp"),
        P(SP, "tp"),
        P(SP, "tp"),
        P(),
        P(None, "tp"),
        P(None, "tp"),
        P(None, "tp"),
        P(),
        P(),
        P("tp", None, None),
        P(None, "tp"),
    )
    return jax.shard_map(body, mesh=split, in_specs=placed, out_specs=P(SP, "tp"), check_vma=False)
```

profile of v0, /device:TPU:1, one launch (start us, length us, event | category | flops | bytes accessed | tf_op | source)
XLA Modules:
  0.0 121.4 jit_solution(677514866326986524)
XLA Ops:
  0.0 0.8 convert_bitcast_fusion
  0.8 0.8 fusion.42
  1.7 0.8 fusion.41
  2.5 0.9 fusion.38
  3.4 20.5 %psum.14 = f32[5,256]{1,0:T(8,128)S(1)} all-reduce(f32[5,256]{1,0:T(8,128)S(1)} %pad_maximum_fusion.2), channel_id=1, replica_groups=mesh['sp_0'=8,'sp_1'=8,'tp'=8] {'sp_0'}, use_global_device_ids=true, to_apply=%region_0.1 | all-reduce | flops 1280 | bytes 10240 | tf_op jit(solution)/shard_map/psum | solution.py:20
  23.9 14.1 %psum.15 = f32[5,256]{1,0:T(8,128)S(1)} all-reduce(f32[5,256]{1,0:T(8,128)S(1)} %psum.14), channel_id=1, replica_groups=mesh['sp_0'=8,'sp_1'=8,'tp'=8] {'sp_1'}, use_global_device_ids=true, to_apply=%region_1.2 | all-reduce | flops 1280 | bytes 10240 | tf_op jit(solution)/shard_map/psum | solution.py:20
  38.0 0.6 broadcast_in_dim.24
  38.6 12.5 %all-to-all-start = ((f32[8,5,256]{2,1,0:T(8,128)}), f32[8,5,256]{2,1,0:T(8,128)S(1)}, u32[]{:S(2)}, u32[]{:S(2)}) async-start(f32[8,5,256]{2,1,0:T(8,128)} %broadcast_in_dim.24), calls=%async_computation | async-start | bytes 131072 | tf_op jit(solution)/shard_map/all_to_all | solution.py:32
  51.3 1.5 %fusion = f32[256]{0:T(256)S(1)} fusion(bf16[256,2048]{1,0:T(8,128)(2,1)} %param.17), kind=kLoop, calls=%fused_computation.3 | loop fusion | flops 1572608 | bytes 1049600 | tf_op jit(solution)/shard_map/reduce_sum | solution.py:61
  52.9 0.9 fusion.25
  53.9 5.6 %convolution_bitcast_fusion = f32[2,15,4,16,32,1]{4,1,5,3,2,0:T(8,128)S(1)} fusion(f32[4,16,32,31,1]{3,2,1,0,4:T(8,128)S(1)} %copy-done.5, f32[2,15,31,1,1]{2,0,1,4,3:T(2,128)} %bitcast.131), kind=kOutput, calls=%fused_computation.20 | convolution fusion | flops 22855680 | bytes 503432 | tf_op jit(solution)/shard_map/hxc,bqkc->hxbqk/dot_general | solution.py:151
  59.5 2.3 %fusion.32 = f32[2,4,16,32,4,8]{3,5,4,2,1,0:T(8,128)} fusion(f32[2,15,4,16,32,1]{4,1,5,3,2,0:T(8,128)S(1)} %convolution_bitcast_fusion, s32[4,8]{1,0:T(4,128)S(1)} %subtract_add_fusion), kind=kOutput, calls=%fused_computation.59 | convolution fusion | flops 23593440 | bytes 770176 | tf_op jit(solution)/shard_map/rjx,hxbqk->rhbqjk/dot_general | solution.py:154
  62.0 0.5 fusion.4
  62.5 0.4 fusion.49
  63.2 0.3 mul.200
  63.8 0.4 convolution_convert_fusion
  64.2 1.8 %collective-permute-start = (bf16[4,2,64,128]{3,2,0,1:T(8,128)(2,1)S(1)}, bf16[4,2,64,128]{3,2,0,1:T(8,128)(2,1)S(1)}, u32[]{:S(2)}, u32[]{:S(2)}) collective-permute-start(bf16[4,2,64,128]{3,2,0,1:T(8,128)(2,1)S(1)} %pad_maximum_fusion.1), channel_id=1, source_target_pairs={{0,8},{8,16},{16,24},{24,32},{32,40},{40,48},{48,56},{56,64},{64,7... | collective-permute-start | bytes 393224 | tf_op jit(solution)/shard_map/ppermute | solution.py:51
  66.0 1.3 %collective-permute-start.1 = (bf16[4,2,64,128]{3,2,0,1:T(8,128)(2,1)S(1)}, bf16[4,2,64,128]{3,2,0,1:T(8,128)(2,1)S(1)}, u32[]{:S(2)}, u32[]{:S(2)}) collective-permute-start(bf16[4,2,64,128]{3,2,0,1:T(8,128)(2,1)S(1)} %pad_maximum_fusion.1), channel_id=1, source_target_pairs={{8,0},{16,8},{24,16},{32,24},{40,32},{48,40},{56,48},{64,56},{72,6... | collective-permute-start | bytes 393224 | tf_op jit(solution)/shard_map/ppermute | solution.py:54
  67.3 0.2 fusion.50
  67.6 0.2 convolution_convert_fusion.1
  67.8 0.5 bitcast_reduce_fusion
  68.8 0.2 reshape.275
  69.1 0.7 broadcast_in_dim.29
  69.8 9.8 %all-to-all-start.1 = ((bf16[64,8,256]{2,1,0:T(8,128)(2,1)}), bf16[64,8,256]{2,1,0:T(8,128)(2,1)}, u32[]{:S(2)}, u32[]{:S(2)}) async-start(bf16[64,8,256]{2,1,0:T(8,128)(2,1)} %broadcast_in_dim.29), calls=%async_computation.1 | async-start | bytes 524288 | tf_op jit(solution)/shard_map/all_to_all | solution.py:32
  79.7 0.7 gather_fusion
  80.6 1.4 %fusion.46 = (bf16[4,8,2,32,128]{4,3,2,1,0:T(8,128)(2,1)S(1)}, bf16[4,8,2,32,128]{4,3,2,1,0:T(8,128)(2,1)}, bf16[4,8,2,32,128]{4,3,2,1,0:T(8,128)(2,1)S(1)}, bf16[4,8,2,32,128]{4,3,2,1,0:T(8,128)(2,1)S(1)}) fusion(bf16[4,8,2,64,128]{4,3,2,1,0:T(8,128)(2,1)S(1)} %broadcast_select_fusion), kind=kLoop, calls=%fused_computation.92 | loop fusion | bytes 4194304 | tf_op jit(solution)/shard_map/slice | solution.py:137
  82.0 0.4 stack.31
  82.4 1.2 copy_dynamic-update-slice_fusion.3
  83.7 0.4 stack.32
  84.1 2.5 %stack.33 = bf16[4,8,2,1,32,2,64]{6,5,4,2,1,0,3:T(2,128)(2,1)S(1)} reshape(bf16[4,8,2,32,128]{4,3,2,1,0:T(8,128)(2,1)} %get-tuple-element.6) | data formatting | bytes 1048576 | tf_op jit(solution)/shard_map/stack | solution.py:137
  86.5 1.4 %stack.34 = bf16[4,8,2,1,32,2,64]{6,5,4,2,1,0,3:T(2,128)(2,1)} reshape(bf16[4,8,2,32,128]{4,3,2,1,0:T(8,128)(2,1)S(1)} %get-tuple-element.5) | data formatting | bytes 1048576 | tf_op jit(solution)/shard_map/stack | solution.py:137
  87.9 1.2 copy_dynamic-update-slice_fusion.2
  89.1 1.2 copy_dynamic-update-slice_fusion.1
  90.3 1.2 copy_dynamic-update-slice_fusion
  91.5 4.5 %fusion.51 = (f32[4,2,4,16]{3,2,1,0:T(4,128)S(1)}, f32[4,2,4,16,8,32]{5,3,4,2,1,0:T(8,128)S(1)}) fusion(f32[2,4,16,32,4,8]{3,5,4,2,1,0:T(8,128)S(1)} %copy-done.1, bf16[4,8,2,4,32,2,64]{6,4,1,3,5,0,2:T(8,128)(2,1)} %copy_dynamic-update-slice_fusion, pred[4,16,32]{2,1,0:T(8,128)(4,1)S(1)} %copy-done.8, f32[64]{0:T(128)S(1)} %convert_element_type.95, ...), kind=kOutput, calls=%fused_computation.97 | convolution fusion | flops 17399296 | bytes 3283200 | tf_op jit(solution)/shard_map/rbqhd,rjbkhd->rhbqjk/dot_general | solution.py:158
  96.1 0.9 copy.124
  96.9 0.6 reshape.302
  97.6 1.0 fusion.47
  98.7 0.4 fusion.52
  99.1 0.5 fusion.18
  99.6 0.4 divide_convert_fusion
  100.0 0.4 reshape.279
  100.4 2.5 %fusion.12 = f32[4,4,16,2,64]{4,2,3,1,0:T(8,128)S(1)} fusion(bf16[4,2,4,16,8,32]{5,4,3,2,0,1:T(8,128)(2,1)S(1)} %reshape.279, bf16[4,8,2,4,32,2,64]{6,4,1,3,5,0,2:T(8,128)(2,1)} %copy_dynamic-update-slice_fusion), kind=kOutput, calls=%fused_computation.23 | convolution fusion | flops 16777216 | bytes 2490368 | tf_op jit(solution)/shard_map/rhbqjk,rjbkhd->rbqhd/dot_general | solution.py:175
  103.0 0.3 fusion.16
  103.6 0.8 broadcast_in_dim.30
  104.5 5.6 %all-to-all-start.2 = ((bf16[8,256,128]{1,2,0:T(8,128)(2,1)}), bf16[8,256,128]{1,2,0:T(8,128)(2,1)S(1)}, u32[]{:S(2)}, u32[]{:S(2)}) async-start(bf16[8,256,128]{1,2,0:T(8,128)(2,1)} %broadcast_in_dim.30), calls=%async_computation.2 | async-start | bytes 1048576 | tf_op jit(solution)/shard_map/all_to_all | solution.py:32
  110.2 9.3 %all-to-all-done.2 = bf16[8,256,128]{1,2,0:T(8,128)(2,1)S(1)} async-done(((bf16[8,256,128]{1,2,0:T(8,128)(2,1)}), bf16[8,256,128]{1,2,0:T(8,128)(2,1)S(1)}, u32[]{:S(2)}, u32[]{:S(2)}) %all-to-all-start.2) | async-done | bytes 524320 | tf_op jit(solution)/shard_map/all_to_all | solution.py:32
  119.5 1.9 %fusion.17 = bf16[256,256]{1,0:T(8,128)(2,1)} fusion(bf16[256,1024]{0,1:T(8,128)(2,1)S(1)} %bitcast.121, bf16[1024,256]{1,0:T(8,128)(2,1)S(1)} %copy-done.10, f32[256]{0:T(256)S(1)} %dynamic_slice.7, bf16[256,2048]{1,0:T(8,128)(2,1)} %param.17, s32[]{:T(128)S(6)} %select_n.28), kind=kOutput, calls=%fused_computation.27 | convolution fusion | flops 134479872 | bytes 1311748 | tf_op jit(solution)/shard_map/dot_general | solution.py:182
  (73 shorter events, 2.4 us)
Async XLA Ops:
  0.0 62.5 %copy-start = (bf16[2048,128]{1,0:T(8,128)(2,1)S(1)}, bf16[2048,128]{1,0:T(8,128)(2,1)}, u32[]{:S(2)}) copy-start(bf16[2048,128]{1,0:T(8,128)(2,1)} %param.26) | copy-start | bytes 1572868
  0.0 53.9 %copy-start.5 = (f32[4,16,32,31,1]{3,2,1,0,4:T(8,128)S(1)}, f32[4,16,32,31,1]{3,2,1,0,4:T(8,128)}, u32[]{:S(2)}) copy-start(f32[4,16,32,31,1]{3,2,1,0,4:T(8,128)} %constant.87) | copy-start | bytes 761860
  38.6 23.3 %all-to-all-start = ((f32[8,5,256]{2,1,0:T(8,128)}), f32[8,5,256]{2,1,0:T(8,128)S(1)}, u32[]{:S(2)}, u32[]{:S(2)}) async-start(f32[8,5,256]{2,1,0:T(8,128)} %broadcast_in_dim.24), calls=%async_computation | async-start | bytes 131072 | tf_op jit(solution)/shard_map/all_to_all | solution.py:32
  59.4 2.4 %copy-start.9 = (bf16[2048]{0:T(1024)(128)(2,1)S(1)}, bf16[2048]{0:T(1024)(128)(2,1)}, u32[]{:S(2)}) copy-start(bf16[2048]{0:T(1024)(128)(2,1)} %param.24) | copy-start | bytes 12292
  59.4 2.4 %copy-start.11 = (bf16[64]{0:T(256)(128)(2,1)S(1)}, bf16[64]{0:T(256)(128)(2,1)}, u32[]{:S(2)}) copy-start(bf16[64]{0:T(256)(128)(2,1)} %param.29) | copy-start | bytes 388
  59.5 2.5 %copy-start.12 = (bf16[64]{0:T(256)(128)(2,1)S(1)}, bf16[64]{0:T(256)(128)(2,1)}, u32[]{:S(2)}) copy-start(bf16[64]{0:T(256)(128)(2,1)} %param.28) | copy-start | bytes 388
  59.5 2.5 %copy-start.2 = (bf16[256,2048]{1,0:T(8,128)(2,1)S(1)}, bf16[256,2048]{1,0:T(8,128)(2,1)}, u32[]{:S(2)}) copy-start(bf16[256,2048]{1,0:T(8,128)(2,1)} %param.17) | copy-start | bytes 3145732
  62.5 1.3 %copy-start.4 = (bf16[2048,128]{1,0:T(8,128)(2,1)S(1)}, bf16[2048,128]{1,0:T(8,128)(2,1)}, u32[]{:S(2)}) copy-start(bf16[2048,128]{1,0:T(8,128)(2,1)} %param.27) | copy-start | bytes 1572868
  62.9 4.4 %copy-start.7 = (bf16[8,2048]{1,0:T(8,128)(2,1)S(1)}, bf16[8,2048]{1,0:T(8,128)(2,1)}, u32[]{:S(2)}) copy-start(bf16[8,2048]{1,0:T(8,128)(2,1)} %param.18) | copy-start | bytes 98308
  63.2 4.6 %copy-start.6 = (bf16[2048,128]{1,0:T(8,128)(2,1)S(1)}, bf16[2048,128]{1,0:T(8,128)(2,1)}, u32[]{:S(2)}) copy-start(bf16[2048,128]{1,0:T(8,128)(2,1)} %param.25) | copy-start | bytes 1572868
  64.2 15.4 %collective-permute-start = (bf16[4,2,64,128]{3,2,0,1:T(8,128)(2,1)S(1)}, bf16[4,2,64,128]{3,2,0,1:T(8,128)(2,1)S(1)}, u32[]{:S(2)}, u32[]{:S(2)}) collective-permute-start(bf16[4,2,64,128]{3,2,0,1:T(8,128)(2,1)S(1)} %pad_maximum_fusion.1), channel_id=1, source_target_pairs={{0,8},{8,16},{16,24},{24,32},{32,40},{40,48},{48,56},{56,64},{64,7... | collective-permute-start | bytes 393224 | tf_op jit(solution)/shard_map/ppermute | solution.py:51
  66.0 13.6 %collective-permute-start.1 = (bf16[4,2,64,128]{3,2,0,1:T(8,128)(2,1)S(1)}, bf16[4,2,64,128]{3,2,0,1:T(8,128)(2,1)S(1)}, u32[]{:S(2)}, u32[]{:S(2)}) collective-permute-start(bf16[4,2,64,128]{3,2,0,1:T(8,128)(2,1)S(1)} %pad_maximum_fusion.1), channel_id=1, source_target_pairs={{8,0},{16,8},{24,16},{32,24},{40,32},{48,40},{56,48},{64,56},{72,6... | collective-permute-start | bytes 393224 | tf_op jit(solution)/shard_map/ppermute | solution.py:54
  69.8 27.7 %all-to-all-start.1 = ((bf16[64,8,256]{2,1,0:T(8,128)(2,1)}), bf16[64,8,256]{2,1,0:T(8,128)(2,1)}, u32[]{:S(2)}, u32[]{:S(2)}) async-start(bf16[64,8,256]{2,1,0:T(8,128)(2,1)} %broadcast_in_dim.29), calls=%async_computation.1 | async-start | bytes 524288 | tf_op jit(solution)/shard_map/all_to_all | solution.py:32
  87.9 2.4 %copy-start.3 = (bf16[4,8,2,1,32,2,64]{6,5,4,2,1,0,3:T(2,128)(2,1)S(1)}, bf16[4,8,2,1,32,2,64]{6,5,4,2,1,0,3:T(2,128)(2,1)}, u32[]{:S(2)}) copy-start(bf16[4,8,2,1,32,2,64]{6,5,4,2,1,0,3:T(2,128)(2,1)} %stack.34) | copy-start | bytes 1572868
  89.1 2.4 %copy-start.1 = (f32[2,4,16,32,4,8]{3,5,4,2,1,0:T(8,128)S(1)}, f32[2,4,16,32,4,8]{3,5,4,2,1,0:T(8,128)}, u32[]{:S(2)}) copy-start(f32[2,4,16,32,4,8]{3,5,4,2,1,0:T(8,128)} %fusion.32) | copy-start | bytes 1572868
  89.1 2.4 %copy-start.8 = (pred[4,16,32]{2,1,0:T(8,128)(4,1)S(1)}, pred[4,16,32]{2,1,0:T(8,128)(4,1)}, u32[]{:S(2)}) copy-start(pred[4,16,32]{2,1,0:T(8,128)(4,1)} %constant.79.clone) | copy-start | bytes 6148
  102.9 16.6 %copy-start.10 = (bf16[1024,256]{1,0:T(8,128)(2,1)S(1)}, bf16[1024,256]{1,0:T(8,128)(2,1)}, u32[]{:S(2)}) copy-start(bf16[1024,256]{1,0:T(8,128)(2,1)} %param.31) | copy-start | bytes 1572868
  104.5 15.0 %all-to-all-start.2 = ((bf16[8,256,128]{1,2,0:T(8,128)(2,1)}), bf16[8,256,128]{1,2,0:T(8,128)(2,1)S(1)}, u32[]{:S(2)}, u32[]{:S(2)}) async-start(bf16[8,256,128]{1,2,0:T(8,128)(2,1)} %broadcast_in_dim.30), calls=%async_computation.2 | async-start | bytes 1048576 | tf_op jit(solution)/shard_map/all_to_all | solution.py:32
where the time goes:
time: 122 us; the launch traced here: 121 us
  blocking collectives  34.6 us (28%)
  starting transfers between devices  31 us (25%)
  matrix products  21.9 us (18%)
  local copies, waits for them, and re-layouts  18.9 us (15%)
  waiting for transfers between devices  9.29 us (8%)
  other arithmetic  5.2 us (4%)
    psum x2, blocking collectives, one_axis_at_a_time(): x = lax.psum(x, axis)  34.6 us
    all_to_all x3, starting transfers between devices, sent_to_all(): return lax.all_to_all(copies, axis, split_axis=0, concat_axis=0, tiled=True)  27.9 us
    all_to_all x3, waiting for transfers between devices, sent_to_all(): return lax.all_to_all(copies, axis, split_axis=0, concat_axis=0, tiled=True)  9.28 us
    another operation x5, local copies, waits for them, and re-layouts, body(): jnp.stack([band[:, :, :, begin:begin + span] for begin in starts], axis=3)  5.84 us
    dot_general x1, matrix products, body(): jnp.einsum('hxc,bqkc->hxbqk', offset_bias, jnp.asarray(col_onehot), preci...  5.56 us
    dot_general x1, matrix products, body(): jnp.einsum('rbqhd,rjbkhd->rhbqjk', grid_q, key_blocks, preferred_element_...  4.53 us
    unnamed x29, local copies, waits for them, and re-layouts  3.67 us
    dot_general x1, matrix products, body(): jnp.einsum('rhbqjk,rjbkhd->rbqhd', local_w, value_blocks, preferred_eleme...  2.47 us
  transfers between devices with their start and end apart: 5, of which 1 were waited for; matrix products, arithmetic and copies ran while one was open for 26% of the time, Pallas kernels for 0%

commit v1 on v0

v1 whole, which is shorter than its diff:
```python
import functools
import math

import jax
import jax.numpy as jnp
from jax import lax
from jax.experimental import pallas as pl
from jax.experimental.pallas import tpu as pltpu
from jax.sharding import Mesh
from jax.sharding import PartitionSpec as P

HEAD_DIM = 64
WIN_ROWS = 8
WIN_COLS = 16
GRID_W = 64
ROWS = 4
TOK = ROWS * GRID_W
LANE = 2 * HEAD_DIM
BLOCK = 256
CTX_DEV = 8
EPS = 1e-06
LOG2E = math.log2(math.e)
NEG = -1e30
SMALL = (2, 3, 7, 11, 12, 13)
AXES = ("z", "y", "x", "c")
MESH = pl.DeviceIdType.MESH
F32 = jnp.float32
BF16 = jnp.bfloat16


def far_first(n):
    return sorted(range(1, n), key=lambda d: -min(d, n - d))


def near_first(n):
    return [0] + sorted(range(1, n), key=lambda d: min(d, n - d))


def dot(a, b):
    return jnp.dot(a, b, preferred_element_type=F32)


def dot_nt(a, b):
    return lax.dot_general(a, b, (((1,), (1,)), ((), ())), preferred_element_type=F32)


def silu(v):
    return v / (1.0 + jnp.exp(-v))


def head_norm(raw, ones_block):
    sq = raw * raw
    hi = sq.astype(BF16)
    lo = (sq - hi.astype(F32)).astype(BF16)
    return raw * lax.rsqrt(dot(hi, ones_block) + dot(lo, ones_block) + EPS)


def kernel(
    sizes,
    latent,
    context,
    cond_hbm,
    cond_ctx_hbm,
    shift_w,
    scale_w,
    gate_w,
    norm_gain_hbm,
    query_w,
    key_w,
    value_w,
    query_gain_hbm,
    key_gain_hbm,
    offset_bias_hbm,
    out_w,
    out,
    lat,
    xn,
    hid,
    w_all,
    wo,
    own,
    craw,
    cxn,
    chid,
    kv,
    kvc,
    qm,
    table,
    top,
    acc,
    bias_rows,
    gains,
    gain_row,
    wmod,
    m1,
    m2,
    g1,
    g2,
    mod,
    mx,
    cond,
    cond_ctx,
    norm_gain,
    query_gain,
    key_gain,
    offset_bias,
    load_sem,
    s1,
    r1,
    s2,
    r2,
    sg1,
    rg1,
    sg2,
    rg2,
    s3,
    r3,
    sc,
    rc,
    sk,
    rk,
    sh,
    rh,
    sm,
    rm,
    sf,
    rf,
):
    nz, ny, nx, nc = sizes
    nsp, ntp = nz * ny, nx * nc
    width = ntp * BLOCK
    ctx_line = ny * CTX_DEV
    z, y, x, c = (lax.axis_index(a) for a in AXES)
    s = z * ny + y
    t = x * nc + c
    sib = 1 - c

    def line(axis, me, d, n):
        return {axis: lax.rem(me + d, n)}

    def tp_peer(dx, dc):
        return {"x": lax.rem(x + dx, nx), "c": lax.rem(c + dc, nc)}

    def sp_peer(step):
        p = lax.rem(s + step + nsp, nsp)
        return {"z": p // ny, "y": lax.rem(p, ny)}

    tp_steps = [(dx, dc) for dx in range(nx) for dc in range(nc) if (dx, dc) != (0, 0)]

    barrier = pltpu.get_barrier_semaphore()
    peers = [line("y", y, d, ny) for d in range(1, ny)]
    peers += [line("z", z, d, nz) for d in range(1, nz)]
    peers += [tp_peer(dx, dc) for dx, dc in tp_steps]
    peers += [sp_peer(1), sp_peer(-1)]
    for peer in peers:
        pl.semaphore_signal(barrier, inc=1, device_id=peer, device_id_type=MESH)

    def load(k, src, dst):
        cp = pltpu.make_async_copy(src, dst, load_sem.at[k])
        cp.start()
        return cp

    first_loads = [
        load(10, cond_hbm, cond),
        load(11, cond_ctx_hbm, cond_ctx),
        load(0, shift_w, wmod.at[0]),
        load(1, scale_w, wmod.at[1]),
        load(2, gate_w, wmod.at[2]),
    ]
    gain_load = load(12, norm_gain_hbm, norm_gain)
    ctx_load = load(3, context, craw.at[0])
    lat_load = load(4, latent, lat)
    bias_load = load(15, offset_bias_hbm, offset_bias)
    w_loads = [
        load(13, query_gain_hbm, query_gain),
        load(14, key_gain_hbm, key_gain),
        load(5, key_w, w_all.at[:, 0:LANE]),
        load(6, value_w, w_all.at[:, LANE : 2 * LANE]),
        load(7, query_w, w_all.at[:, 2 * LANE : 3 * LANE]),
    ]
    late_loads = [
        load(8, latent.at[:, pl.ds(pl.multiple_of(t * BLOCK, BLOCK), BLOCK)], own),
        load(9, out_w, wo),
    ]

    for cp in first_loads:
        cp.wait()
    act = silu(cond[...].astype(F32)).astype(BF16)
    act_ctx = silu(cond_ctx[...].astype(F32)).astype(BF16)
    acts = jnp.concatenate([act, act_ctx], axis=0)
    p_shift = dot(acts, wmod[0])
    p_scale = dot(acts, wmod[1])
    p_gate = dot(acts, wmod[2])
    half = BLOCK // 2
    m1[0, 0:2, :] = p_shift[:, :half]
    m1[0, 2:4, :] = p_scale[:, :half]
    m1[0, 4:6, :] = p_shift[:, half:]
    m1[0, 6:8, :] = p_scale[:, half:]
    g1[0, 0:2, :] = p_gate[:, :half]
    g1[0, 2:4, :] = p_gate[:, half:]
    g1[0, 4:8, :] = jnp.zeros((4, half), F32)
    ctx_load.wait()
    pl.semaphore_wait(barrier, len(peers))

    def remote(src, dst, send, recv, peer):
        return pltpu.make_async_remote_copy(
            src_ref=src,
            dst_ref=dst,
            send_sem=send,
            recv_sem=recv,
            device_id=peer,
            device_id_type=MESH,
        )

    sent = []

    def send_line(axis, me, n, src, dst_of, send, recv):
        copies = {}
        for d in far_first(n):
            cp = remote(src, dst_of(d), send.at[d], recv.at[d], line(axis, me, d, n))
            cp.start()
            copies[d] = cp
        sent.extend(copies.values())
        return copies

    p1 = send_line("y", y, ny, m1.at[0], lambda d: m1.at[d], s1, r1)
    pc = send_line("y", y, ny, craw.at[0], lambda d: craw.at[d], sc, rc)
    pg1 = send_line("y", y, ny, g1.at[0], lambda d: g1.at[d], sg1, rg1)

    gain_load.wait()
    for b in range(width // LANE):
        gain_row[0:1, b * LANE : (b + 1) * LANE] = norm_gain[b : b + 1, :].astype(F32)
    gain = gain_row[...]
    lat_load.wait()

    def norm_rows(i, carry):
        rows = pl.ds(pl.multiple_of(i * 16, 16), 16)
        v = lat[rows, :].astype(F32)
        r = lax.rsqrt(jnp.mean(v * v, axis=-1, keepdims=True) + EPS)
        xn[rows, :] = v * r * gain
        return carry

    lax.fori_loop(0, TOK // 16, norm_rows, 0)

    for cp in p1.values():
        cp.wait_recv()
    total = m1[0]
    for d in range(1, ny):
        total = total + m1[d]
    m2[0] = total
    p2 = send_line("z", z, nz, m2.at[0], lambda d: m2.at[d], s2, r2)

    bias_load.wait()
    bias_rows[...] = jnp.zeros(bias_rows.shape, F32)
    for h in range(2):
        bias_rows[h, 0 : 2 * WIN_ROWS - 1, 0 : 2 * WIN_COLS - 1] = offset_bias[:, h, :]
    kv[:, 2 * LANE :] = jnp.ones((3 * TOK, LANE), BF16)
    kvc[:, 2 * LANE :] = jnp.ones((kvc.shape[0], LANE), BF16)
    q_col = lax.broadcasted_iota(jnp.int32, (GRID_W, LANE), 0)
    lane = lax.broadcasted_iota(jnp.int32, (GRID_W, LANE), 1)
    k_col = lax.rem(lane, GRID_W)
    k_row = lane // GRID_W
    first_col = jnp.clip(q_col - WIN_COLS // 2, 0, GRID_W - WIN_COLS)
    col_ok = (k_col >= first_col) & (k_col < first_col + WIN_COLS)
    for h in range(2):
        table_rows = bias_rows[h]
        pairs = table_rows[0:15] + pltpu.roll(table_rows, GRID_W, 1)[1:16]
        toeplitz = {}
        for ro in range(14):
            spread = jnp.broadcast_to(pairs[ro : ro + 1], (GRID_W, LANE))
            toeplitz[ro] = pltpu.roll(
                spread, LANE - (WIN_COLS - 1), 1, stride=1, stride_axis=0
            )
        for r in range(ROWS):
            begin = jnp.where(s == 0, ROWS, jnp.where(s == nsp - 1, 0, r))
            rows = pl.ds(h * TOK + r * GRID_W, GRID_W)
            high = None
            tiles = []
            for kp in range(6):
                row = k_row + 2 * kp
                ok = col_ok & (row >= begin) & (row < begin + WIN_ROWS)
                tile = jnp.where(ok, toeplitz[2 * kp - r + 3], NEG)
                tiles.append(tile)
                high = tile if high is None else jnp.maximum(high, tile)
            peak = jnp.max(high, axis=-1, keepdims=True)
            top[rows, :] = jnp.broadcast_to(peak * LOG2E, (GRID_W, LANE))
            for kp in range(6):
                table[rows, kp * LANE : (kp + 1) * LANE] = (tiles[kp] - peak) * LOG2E

    for cp in p2.values():
        cp.wait_recv()
    total = m2[0]
    for d in range(1, nz):
        total = total + m2[d]
    mod[t] = total
    p3 = {}
    for dx, dc in tp_steps:
        k = dx * nc + dc
        cp = remote(mod.at[t], mod.at[t], s3.at[k], r3.at[k], tp_peer(dx, dc))
        cp.start()
        sent.append(cp)
        src = lax.rem(x + nx - dx, nx) * nc + lax.rem(c + nc - dc, nc)
        p3[k] = remote(mod.at[src], mod.at[src], s3.at[k], r3.at[k], tp_peer(dx, dc))

    for cp in pc.values():
        cp.wait_recv()
    for d in range(ny):
        v = craw[d].astype(F32)
        r = lax.rsqrt(jnp.mean(v * v, axis=-1, keepdims=True) + EPS)
        cxn[d * CTX_DEV : (d + 1) * CTX_DEV, :] = v * r * gain
    for cp in pg1.values():
        cp.wait_recv()
    total = g1[0]
    for d in range(1, ny):
        total = total + g1[d]
    g2[0] = total
    pg2 = send_line("z", z, nz, g2.at[0], lambda d: g2.at[d], sg2, rg2)

    row_head = lax.broadcasted_iota(jnp.int32, (LANE, LANE), 0) // HEAD_DIM
    col_head = lax.broadcasted_iota(jnp.int32, (LANE, LANE), 1) // HEAD_DIM
    ones_block = jnp.where(row_head == col_head, 1.0 / HEAD_DIM, 0.0).astype(BF16)
    for cp in w_loads:
        cp.wait()
    kg = key_gain[...].astype(F32)
    qg = query_gain[...].astype(F32) * (HEAD_DIM**-0.5 * LOG2E)
    gains[0:1, 0:HEAD_DIM] = kg
    gains[0:1, HEAD_DIM:LANE] = kg
    gains[1:2, 0:HEAD_DIM] = qg
    gains[1:2, HEAD_DIM:LANE] = qg

    for cp in p3.values():
        cp.wait_recv()

    def vec(block, which):
        return jnp.concatenate([mod[block, which : which + 1, :], mod[block, which + 4 : which + 5, :]], axis=1)

    for b in range(ntp):
        cols = slice(b * BLOCK, (b + 1) * BLOCK)
        chid[:, cols] = (cxn[:, cols] * (1.0 + vec(b, 3)) + vec(b, 1)).astype(BF16)
    raw = dot(chid[...], w_all[:, 0 : 2 * LANE])
    kvc[0:ctx_line, 0:LANE] = (head_norm(raw[:, :LANE], ones_block) * gains[0:1, :]).astype(BF16)
    kvc[0:ctx_line, LANE : 2 * LANE] = raw[:, LANE:].astype(BF16)
    order = near_first(nz)
    place = {d: order.index(d) * ctx_line for d in order}

    def kvc_at(d):
        return kvc.at[place[d] : place[d] + ctx_line, 0 : 2 * LANE]

    pk = send_line("z", z, nz, kvc_at(0), kvc_at, sk, rk)

    for b in range(ntp):
        cols = slice(b * BLOCK, (b + 1) * BLOCK)
        hid[:, cols] = (xn[:, cols] * (1.0 + vec(b, 2)) + vec(b, 0)).astype(BF16)
    raw = dot(hid[...], w_all[:, 0 : 2 * LANE])
    kv[TOK : 2 * TOK, 0:LANE] = (head_norm(raw[:, :LANE], ones_block) * gains[0:1, :]).astype(BF16)
    kv[TOK : 2 * TOK, LANE : 2 * LANE] = raw[:, LANE:].astype(BF16)
    mine = kv.at[TOK : 2 * TOK, 0 : 2 * LANE]
    up = remote(mine, kv.at[0:TOK, 0 : 2 * LANE], sh.at[0], rh.at[0], sp_peer(1))
    down = remote(mine, kv.at[2 * TOK : 3 * TOK, 0 : 2 * LANE], sh.at[1], rh.at[1], sp_peer(-1))
    up.start()
    down.start()
    sent.extend([up, down])

    raw = dot(hid[...], w_all[:, 2 * LANE : 3 * LANE])
    queries = head_norm(raw, ones_block) * gains[1:2, :]
    head_of = lax.broadcasted_iota(jnp.int32, (TOK, LANE), 1) // HEAD_DIM
    for h in range(2):
        qm[h] = jnp.where(head_of == h, queries, 0.0).astype(BF16)

    def window(block, start):
        rows = slice(block * TOK, (block + 1) * TOK)
        for h in range(2):
            sc_ = dot_nt(qm[h], kv[rows, 0:LANE])
            w = jnp.exp2(sc_ + table[h * TOK : (h + 1) * TOK, rows]).astype(BF16)
            part = dot(w, kv[rows, LANE:])
            acc[h] = part if start else acc[h] + part

    def prefix(lo, hi):
        for h in range(2):
            sc_ = dot_nt(qm[h], kvc[lo:hi, 0:LANE])
            peak = top[h * TOK : (h + 1) * TOK, :]
            if hi - lo >= LANE:
                peak = jnp.concatenate([peak] * ((hi - lo) // LANE), axis=1)
            else:
                peak = peak[:, : hi - lo]
            w = jnp.exp2(sc_ - peak).astype(BF16)
            acc[h] = acc[h] + dot(w, kvc[lo:hi, LANE:])

    window(1, True)
    up.wait_recv()
    window(0, False)
    down.wait_recv()
    window(2, False)
    per = max(1, min(BLOCK // ctx_line, nz))
    for g in range(0, nz, per):
        for d in order[g : g + per]:
            if d:
                pk[d].wait_recv()
        prefix(g * ctx_line, (g + per) * ctx_line)

    parts = []
    for h in range(2):
        full = acc[h]
        parts.append(full[:, :LANE] / full[:, LANE:])
    mx[0, c] = jnp.where(head_of == 0, parts[0], parts[1]).astype(BF16)

    mine = mx.at[0, c]
    pm = {}
    for dx in far_first(nx):
        cp = remote(mine, mx.at[dx, c], sm.at[dx], rm.at[dx], tp_peer(dx, 0))
        cp.start()
        pm[dx] = cp
    sent.extend(pm.values())
    pf = {}
    for dx in range(nx):
        pf[dx] = remote(mx.at[dx, c], mx.at[dx, c], sf.at[dx], rf.at[dx], {"c": sib})
    got = {dx: remote(mx.at[dx, sib], mx.at[dx, sib], sf.at[dx], rf.at[dx], {"c": sib}) for dx in range(nx)}
    pf[0].start()
    sent.extend(pf.values())

    for cp in pg2.values():
        cp.wait_recv()
    total = g2[0]
    for d in range(1, nz):
        total = total + g2[d]
    gate = jnp.concatenate([total[0:1], total[2:3]], axis=1)
    for cp in late_loads:
        cp.wait()
    for dx in sorted(range(1, nx), key=lambda d: min(d, nx - d)):
        pm[dx].wait_recv()
        pf[dx].start()
    proj = None
    for dx in [0] + sorted(range(1, nx), key=lambda d: min(d, nx - d)):
        got[dx].wait_recv()
        src = lax.rem(x + nx - dx, nx)
        rows = pl.ds(pl.multiple_of(src * 2 * LANE, 2 * LANE), 2 * LANE)
        part = dot(jnp.concatenate([mx[dx, 0], mx[dx, 1]], axis=1), wo[rows, :])
        proj = part if proj is None else proj + part
    out[...] = (own[...].astype(F32) + gate * proj).astype(BF16)
    for cp in sent:
        cp.wait_send()


def solution(mesh):
    nsp, ntp = mesh.devices.shape
    sizes = SIZES if SIZES else (8, nsp // 8, ntp // 2, 2)
    nz, ny, nx, nc = sizes
    split = Mesh(mesh.devices.reshape(sizes), AXES)
    sp, tp = ("z", "y"), ("x", "c")
    placed = (
        P(sp, None),
        P(sp, None),
        P(sp),
        P(sp),
        P(sp, tp),
        P(sp, tp),
        P(sp, tp),
        P(),
        P(None, tp),
        P(None, tp),
        P(None, tp),
        P(),
        P(),
        P(tp, None, None),
        P(None, tp),
    )
    width = ntp * BLOCK
    ctx_line = ny * CTX_DEV
    dma = pltpu.SemaphoreType.DMA
    vm = pltpu.VMEM

    def body(
        latent,
        context,
        cond,
        cond_ctx,
        shift_w,
        scale_w,
        gate_w,
        norm_gain,
        query_w,
        key_w,
        value_w,
        query_gain,
        key_gain,
        offset_bias,
        out_w,
    ):
        args = [
            latent,
            context,
            cond.reshape(1, -1),
            cond_ctx.reshape(1, -1),
            shift_w,
            scale_w,
            gate_w,
            norm_gain.reshape(-1, LANE),
            query_w,
            key_w,
            value_w,
            query_gain.reshape(1, -1),
            key_gain.reshape(1, -1),
            jnp.transpose(offset_bias, (1, 0, 2)),
            out_w,
        ]
        specs = [pl.BlockSpec(memory_space=pltpu.HBM)] * len(args)
        small = [vm(args[i].shape, args[i].dtype) for i in SMALL]
        depth = shift_w.shape[0]
        scratch = [
            vm((TOK, width), BF16),
            vm((TOK, width), F32),
            vm((TOK, width), BF16),
            vm((width, 3 * LANE), BF16),
            vm((ntp * LANE, BLOCK), BF16),
            vm((TOK, BLOCK), BF16),
            vm((ny, CTX_DEV, width), BF16),
            vm((ctx_line, width), F32),
            vm((ctx_line, width), BF16),
            vm((3 * TOK, 3 * LANE), BF16),
            vm((nz * ctx_line, 3 * LANE), BF16),
            vm((2, TOK, LANE), BF16),
            vm((2 * TOK, 3 * TOK), F32),
            vm((2 * TOK, LANE), F32),
            vm((2, TOK, 2 * LANE), F32),
            vm((2, 16, LANE), F32),
            vm((2, LANE), F32),
            vm((1, width), F32),
            vm((3, depth, BLOCK), BF16),
            vm((ny, 8, LANE), F32),
            vm((nz, 8, LANE), F32),
            vm((ny, 8, LANE), F32),
            vm((nz, 8, LANE), F32),
            vm((ntp, 8, LANE), F32),
            vm((nx, 2, TOK, LANE), BF16),
            *small,
            dma((16,)),
            dma((ny,)),
            dma((ny,)),
            dma((nz,)),
            dma((nz,)),
            dma((ny,)),
            dma((ny,)),
            dma((nz,)),
            dma((nz,)),
            dma((ntp,)),
            dma((ntp,)),
            dma((ny,)),
            dma((ny,)),
            dma((nz,)),
            dma((nz,)),
            dma((2,)),
            dma((2,)),
            dma((nx,)),
            dma((nx,)),
            dma((nx,)),
            dma((nx,)),
        ]
        return pl.pallas_call(
            functools.partial(kernel, sizes),
            out_shape=jax.ShapeDtypeStruct((TOK, BLOCK), BF16),
            in_specs=specs,
            out_specs=pl.BlockSpec(memory_space=pltpu.VMEM),
            scratch_shapes=scratch,
            compiler_params=pltpu.CompilerParams(
                collective_id=0, has_side_effects=True, vmem_limit_bytes=63 * 1024 * 1024
            ),
            name="fused_layer",
        )(*args)

    return jax.shard_map(body, mesh=split, in_specs=placed, out_specs=P(sp, tp), check_vma=False)


SIZES = None
```

time: 122 us -> 51.5 us (0.42)
  Pallas kernels: 0 us -> 49.8 us
  blocking collectives: 34.6 us -> 0 us
  starting transfers between devices: 31 us -> 0 us
  matrix products: 21.9 us -> 0 us
  local copies, waits for them, and re-layouts: 18.9 us -> 1.57 us
  waiting for transfers between devices: 9.29 us -> 0 us
  other arithmetic: 5.2 us -> 0 us
    pallas_call x0 -> x1, Pallas kernels: none -> 49.8 us  [body(): pl.pallas_call(functools.partial(kernel, sizes), out_shape=jax.ShapeDtype...]
    psum x2 -> x0, blocking collectives: 34.6 us -> none  [one_axis_at_a_time(): x = lax.psum(x, axis)]
    all_to_all x3 -> x0, starting transfers between devices: 27.9 us -> none  [sent_to_all(): return lax.all_to_all(copies, axis, split_axis=0, concat_axis=0, tiled=True)]
    dot_general x15 -> x0, matrix products: 21.9 us -> none  [the longest x1 5.56 us: body(): jnp.einsum('hxc,bqkc->hxbqk', offset_bias, jnp.asarray(col_onehot), preci...]
    all_to_all x3 -> x0, waiting for transfers between devices: 9.28 us -> none  [sent_to_all(): return lax.all_to_all(copies, axis, split_axis=0, concat_axis=0, tiled=True)]
    another operation x5 -> x0, local copies, waits for them, and re-layouts: 5.84 us -> none  [body(): jnp.stack([band[:, :, :, begin:begin + span] for begin in starts], axis=3)]
    ppermute x2 -> x0, starting transfers between devices: 3.06 us -> none  [the longest x1 1.77 us: padded_2(): lax.ppermute(lax.slice_in_dim(block, block.shape[dim] - width, None, axis...]
    reduce_sum x5 -> x0, other arithmetic: 2.99 us -> none  [the longest x2 2.41 us: modulate(): jnp.mean(values * values, axis=-1, keepdims=True) + EPS]
  transfers between devices with their start and end apart: 5 -> 0, of which waited for: 1 -> 0; matrix products, arithmetic and copies ran while one was open for 26% -> 0% of each run, Pallas kernels for 0% -> 0%
where the time goes in v1:
time: 51.5 us; the launch traced here: 51.4 us
  Pallas kernels  49.8 us (97%)
  local copies, waits for them, and re-layouts  1.57 us (3%)
    pallas_call x1, Pallas kernels, body(): pl.pallas_call(functools.partial(kernel, sizes), out_shape=jax.ShapeDtype...  49.8 us
    unnamed x1, local copies, waits for them, and re-layouts  1.57 us

profile of v1, /device:TPU:1, one launch (start us, length us, event | category | flops | bytes accessed | tf_op | source)
XLA Modules:
  0.0 51.4 jit_solution(12025361143464688046)
XLA Ops:
  0.0 49.8 %fused_layer.1 = bf16[256,256]{1,0:T(8,128)(2,1)} custom-call(bf16[256,2048]{1,0:T(8,128)(2,1)} %latent.1, bf16[8,2048]{1,0:T(8,128)(2,1)} %context.1, bf16[1,32]{1,0:T(2,128)(2,1)} %bitcast.8, bf16[1,32]{1,0:T(2,128)(2,1)} %bitcast.9, bf16[32,256]{1,0:T(8,128)(2,1)} %shift_w.1, bf16[32,256]{1,0:T(8,128)(2,1)} %scale_w.1, bf16[32,256]{1,0:T(8,128)(2,1)} %gate_w.1, ...), custom_call_target="tpu_custom_call" | custom-call | tf_op jit(solution)/shard_map/fused_layer/pallas_call | solution.py:558
  49.8 1.6 %copy.17 = bf16[256,256]{1,0:T(8,128)(2,1)} copy(bf16[256,256]{1,0:T(8,128)(2,1)} %fused_layer.1) | data formatting | bytes 262144

commit v2 on v1

--- a/solution.py
+++ b/solution.py
@@ -26,6 +26,10 @@
 MESH = pl.DeviceIdType.MESH
 F32 = jnp.float32
 BF16 = jnp.bfloat16
+
+
+CLASS_FROM = ((0, 0), (1, 0), (-1, 0), (0, 1), (2, 0), (-2, 0), (1, -1), (-1, 1))
+CLASS = 8
 
 
 def far_first(n):
@@ -126,10 +130,19 @@
     sf,
     rf,
 ):
+    scope = [None]
+
+    def phase(name):
+        if scope[0] is not None:
+            scope[0].__exit__(None, None, None)
+        scope[0] = jax.named_scope(name) if name else None
+        if name:
+            scope[0].__enter__()
+
     nz, ny, nx, nc = sizes
     nsp, ntp = nz * ny, nx * nc
     width = ntp * BLOCK
-    ctx_line = ny * CTX_DEV
+    ctx_line = CLASS * CTX_DEV
     z, y, x, c = (lax.axis_index(a) for a in AXES)
     s = z * ny + y
     t = x * nc + c
@@ -147,6 +160,7 @@
 
     tp_steps = [(dx, dc) for dx in range(nx) for dc in range(nc) if (dx, dc) != (0, 0)]
 
+    phase("greet")
     barrier = pltpu.get_barrier_semaphore()
     peers = [line("y", y, d, ny) for d in range(1, ny)]
     peers += [line("z", z, d, nz) for d in range(1, nz)]
@@ -183,6 +197,7 @@
         load(9, out_w, wo),
     ]
 
+    phase("partial")
     for cp in first_loads:
         cp.wait()
     act = silu(cond[...].astype(F32)).astype(BF16)
@@ -200,6 +215,7 @@
     g1[0, 2:4, :] = p_gate[:, half:]
     g1[0, 4:8, :] = jnp.zeros((4, half), F32)
     ctx_load.wait()
+    phase("barrier")
     pl.semaphore_wait(barrier, len(peers))
 
     def remote(src, dst, send, recv, peer):
@@ -223,10 +239,18 @@
         sent.extend(copies.values())
         return copies
 
+    phase("send1")
     p1 = send_line("y", y, ny, m1.at[0], lambda d: m1.at[d], s1, r1)
-    pc = send_line("y", y, ny, craw.at[0], lambda d: craw.at[d], sc, rc)
-    pg1 = send_line("y", y, ny, g1.at[0], lambda d: g1.at[d], sg1, rg1)
-
+    half_cols = pl.ds(pl.multiple_of(c * (width // 2), width // 2), width // 2)
+
+    def raw_at(slot):
+        return craw.at[slot, :, half_cols]
+
+    across = remote(raw_at(0), raw_at(CLASS), sc.at[0], rc.at[0], line("z", z, nz // 2, nz))
+    across.start()
+    sent.append(across)
+
+    phase("norm")
     gain_load.wait()
     for b in range(width // LANE):
         gain_row[0:1, b * LANE : (b + 1) * LANE] = norm_gain[b : b + 1, :].astype(F32)
@@ -242,6 +266,7 @@
 
     lax.fori_loop(0, TOK // 16, norm_rows, 0)
 
+    phase("wait1")
     for cp in p1.values():
         cp.wait_recv()
     total = m1[0]
@@ -250,12 +275,33 @@
     m2[0] = total
     p2 = send_line("z", z, nz, m2.at[0], lambda d: m2.at[d], s2, r2)
 
+    phase("bias")
+    across.wait_recv()
+    pc = []
+    for d in (4, 3, 5, 2, 6, 1, 7):
+        slot = d // 2 if d % 2 == 0 else 4 + d // 2
+        src = raw_at(0) if d % 2 == 0 else raw_at(CLASS)
+        cp = remote(src, raw_at(slot), sc.at[d], rc.at[d], line("y", y, d, ny))
+        cp.start()
+        pc.append(cp)
+    sent.extend(pc)
+    pg1 = send_line("y", y, ny, g1.at[0], lambda d: g1.at[d], sg1, rg1)
+
     bias_load.wait()
     bias_rows[...] = jnp.zeros(bias_rows.shape, F32)
     for h in range(2):
         bias_rows[h, 0 : 2 * WIN_ROWS - 1, 0 : 2 * WIN_COLS - 1] = offset_bias[:, h, :]
     kv[:, 2 * LANE :] = jnp.ones((3 * TOK, LANE), BF16)
     kvc[:, 2 * LANE :] = jnp.ones((kvc.shape[0], LANE), BF16)
+
+    def clear(when, lo, hi):
+        @pl.when(when)
+        def _():
+            kv[lo:hi, 0 : 2 * LANE] = jnp.zeros((hi - lo, 2 * LANE), BF16)
+
+    clear(s == 0, 0, TOK)
+    clear(s == nsp - 1, 2 * TOK, 3 * TOK - GRID_W)
+    clear(s != 0, 3 * TOK - GRID_W, 3 * TOK)
     q_col = lax.broadcasted_iota(jnp.int32, (GRID_W, LANE), 0)
     lane = lax.broadcasted_iota(jnp.int32, (GRID_W, LANE), 1)
     k_col = lax.rem(lane, GRID_W)
@@ -287,6 +333,7 @@
             for kp in range(6):
                 table[rows, kp * LANE : (kp + 1) * LANE] = (tiles[kp] - peak) * LOG2E
 
+    phase("wait2")
     for cp in p2.values():
         cp.wait_recv()
     total = m2[0]
@@ -302,12 +349,8 @@
         src = lax.rem(x + nx - dx, nx) * nc + lax.rem(c + nc - dc, nc)
         p3[k] = remote(mod.at[src], mod.at[src], s3.at[k], r3.at[k], tp_peer(dx, dc))
 
-    for cp in pc.values():
-        cp.wait_recv()
-    for d in range(ny):
-        v = craw[d].astype(F32)
-        r = lax.rsqrt(jnp.mean(v * v, axis=-1, keepdims=True) + EPS)
-        cxn[d * CTX_DEV : (d + 1) * CTX_DEV, :] = v * r * gain
+    phase("ctxnorm")
+    phase("gate1")
     for cp in pg1.values():
         cp.wait_recv()
     total = g1[0]
@@ -328,39 +371,66 @@
     gains[1:2, 0:HEAD_DIM] = qg
     gains[1:2, HEAD_DIM:LANE] = qg
 
+    phase("wait3")
     for cp in p3.values():
         cp.wait_recv()
 
+    phase("ctxfwd")
+    for cp in pc:
+        cp.wait_recv()
+    sib_cols = pl.ds(pl.multiple_of(sib * (width // 2), width // 2), width // 2)
+    halves = [craw.at[1:CLASS, :, cols] for cols in (half_cols, sib_cols)]
+    cross = remote(halves[0], halves[0], sc.at[8], rc.at[8], {"c": sib})
+    crossed = remote(halves[1], halves[1], sc.at[8], rc.at[8], {"c": sib})
+    cross.start()
+    sent.append(cross)
+
     def vec(block, which):
         return jnp.concatenate([mod[block, which : which + 1, :], mod[block, which + 4 : which + 5, :]], axis=1)
 
+    phase("kv")
+    for b in range(ntp):
+        cols = slice(b * BLOCK, (b + 1) * BLOCK)
+        hid[:, cols] = (xn[:, cols] * (1.0 + vec(b, 2)) + vec(b, 0)).astype(BF16)
+    raw = dot(hid[...], w_all[:, 0 : 2 * LANE])
+    kv[TOK : 2 * TOK, 0:LANE] = (head_norm(raw[:, :LANE], ones_block) * gains[0:1, :]).astype(BF16)
+    kv[TOK : 2 * TOK, LANE : 2 * LANE] = raw[:, LANE:].astype(BF16)
+    def kv_rows(lo, hi):
+        return kv.at[lo:hi, 0 : 2 * LANE]
+
+    short = TOK - GRID_W
+    up = remote(kv_rows(TOK, 2 * TOK), kv_rows(0, TOK), sh.at[0], rh.at[0], sp_peer(1))
+    down = remote(kv_rows(TOK, TOK + short), kv_rows(2 * TOK, 2 * TOK + short), sh.at[1], rh.at[1], sp_peer(-1))
+    last = remote(kv_rows(TOK + short, 2 * TOK), kv_rows(2 * TOK + short, 3 * TOK), sh.at[2], rh.at[2], sp_peer(-1))
+    pl.when(s < nsp - 1)(up.start)
+    pl.when(s > 0)(down.start)
+    pl.when(s == 1)(last.start)
+
+    phase("ctxkv")
+    crossed.wait_recv()
+    for d in range(CLASS):
+        v = craw[d].astype(F32)
+        r = lax.rsqrt(jnp.mean(v * v, axis=-1, keepdims=True) + EPS)
+        cxn[d * CTX_DEV : (d + 1) * CTX_DEV, :] = v * r * gain
     for b in range(ntp):
         cols = slice(b * BLOCK, (b + 1) * BLOCK)
         chid[:, cols] = (cxn[:, cols] * (1.0 + vec(b, 3)) + vec(b, 1)).astype(BF16)
     raw = dot(chid[...], w_all[:, 0 : 2 * LANE])
     kvc[0:ctx_line, 0:LANE] = (head_norm(raw[:, :LANE], ones_block) * gains[0:1, :]).astype(BF16)
     kvc[0:ctx_line, LANE : 2 * LANE] = raw[:, LANE:].astype(BF16)
-    order = near_first(nz)
-    place = {d: order.index(d) * ctx_line for d in order}
-
-    def kvc_at(d):
-        return kvc.at[place[d] : place[d] + ctx_line, 0 : 2 * LANE]
-
-    pk = send_line("z", z, nz, kvc_at(0), kvc_at, sk, rk)
-
-    for b in range(ntp):
-        cols = slice(b * BLOCK, (b + 1) * BLOCK)
-        hid[:, cols] = (xn[:, cols] * (1.0 + vec(b, 2)) + vec(b, 0)).astype(BF16)
-    raw = dot(hid[...], w_all[:, 0 : 2 * LANE])
-    kv[TOK : 2 * TOK, 0:LANE] = (head_norm(raw[:, :LANE], ones_block) * gains[0:1, :]).astype(BF16)
-    kv[TOK : 2 * TOK, LANE : 2 * LANE] = raw[:, LANE:].astype(BF16)
-    mine = kv.at[TOK : 2 * TOK, 0 : 2 * LANE]
-    up = remote(mine, kv.at[0:TOK, 0 : 2 * LANE], sh.at[0], rh.at[0], sp_peer(1))
-    down = remote(mine, kv.at[2 * TOK : 3 * TOK, 0 : 2 * LANE], sh.at[1], rh.at[1], sp_peer(-1))
-    up.start()
-    down.start()
-    sent.extend([up, down])
-
+
+    def kvc_at(k):
+        return kvc.at[k * ctx_line : (k + 1) * ctx_line, 0 : 2 * LANE]
+
+    pk = {}
+    for k in (4, 5, 6, 7, 1, 2, 3):
+        oz, oy = CLASS_FROM[k]
+        peer = {"z": lax.rem(z - oz + nz, nz), "y": lax.rem(y - oy + ny, ny)}
+        pk[k] = remote(kvc_at(0), kvc_at(k), sk.at[k], rk.at[k], peer)
+        pk[k].start()
+    sent.extend(pk.values())
+
+    phase("q")
     raw = dot(hid[...], w_all[:, 2 * LANE : 3 * LANE])
     queries = head_norm(raw, ones_block) * gains[1:2, :]
     head_of = lax.broadcasted_iota(jnp.int32, (TOK, LANE), 1) // HEAD_DIM
@@ -386,18 +456,25 @@
             w = jnp.exp2(sc_ - peak).astype(BF16)
             acc[h] = acc[h] + dot(w, kvc[lo:hi, LANE:])
 
+    phase("attn_own")
     window(1, True)
-    up.wait_recv()
+    phase("attn_up")
+    pl.when(s > 0)(up.wait_recv)
     window(0, False)
-    down.wait_recv()
+    phase("attn_down")
+    pl.when(s < nsp - 1)(down.wait_recv)
+    pl.when(s == 0)(last.wait_recv)
     window(2, False)
-    per = max(1, min(BLOCK // ctx_line, nz))
-    for g in range(0, nz, per):
-        for d in order[g : g + per]:
-            if d:
-                pk[d].wait_recv()
-        prefix(g * ctx_line, (g + per) * ctx_line)
-
+    phase("attn_near")
+    for k in (1, 2, 3):
+        pk[k].wait_recv()
+    prefix(0, 4 * ctx_line)
+    phase("attn_far")
+    for k in (4, 5, 6, 7):
+        pk[k].wait_recv()
+    prefix(4 * ctx_line, CLASS * ctx_line)
+
+    phase("mixed")
     parts = []
     for h in range(2):
         full = acc[h]
@@ -418,6 +495,7 @@
     pf[0].start()
     sent.extend(pf.values())
 
+    phase("gate2")
     for cp in pg2.values():
         cp.wait_recv()
     total = g2[0]
@@ -426,9 +504,11 @@
     gate = jnp.concatenate([total[0:1], total[2:3]], axis=1)
     for cp in late_loads:
         cp.wait()
+    phase("forward")
     for dx in sorted(range(1, nx), key=lambda d: min(d, nx - d)):
         pm[dx].wait_recv()
         pf[dx].start()
+    phase("proj")
     proj = None
     for dx in [0] + sorted(range(1, nx), key=lambda d: min(d, nx - d)):
         got[dx].wait_recv()
@@ -437,8 +517,13 @@
         part = dot(jnp.concatenate([mx[dx, 0], mx[dx, 1]], axis=1), wo[rows, :])
         proj = part if proj is None else proj + part
     out[...] = (own[...].astype(F32) + gate * proj).astype(BF16)
+    phase("drain")
+    pl.when(s < nsp - 1)(up.wait_send)
+    pl.when(s > 0)(down.wait_send)
+    pl.when(s == 1)(last.wait_send)
     for cp in sent:
         cp.wait_send()
+    phase(None)
 
 
 def solution(mesh):
@@ -465,7 +550,7 @@
         P(None, tp),
     )
     width = ntp * BLOCK
-    ctx_line = ny * CTX_DEV
+    ctx_line = CLASS * CTX_DEV
     dma = pltpu.SemaphoreType.DMA
     vm = pltpu.VMEM
 
@@ -513,11 +598,11 @@
             vm((width, 3 * LANE), BF16),
             vm((ntp * LANE, BLOCK), BF16),
             vm((TOK, BLOCK), BF16),
-            vm((ny, CTX_DEV, width), BF16),
+            vm((CLASS + 1, CTX_DEV, width), BF16),
             vm((ctx_line, width), F32),
             vm((ctx_line, width), BF16),
             vm((3 * TOK, 3 * LANE), BF16),
-            vm((nz * ctx_line, 3 * LANE), BF16),
+            vm((CLASS * ctx_line, 3 * LANE), BF16),
             vm((2, TOK, LANE), BF16),
             vm((2 * TOK, 3 * TOK), F32),
             vm((2 * TOK, LANE), F32),
@@ -544,12 +629,12 @@
             dma((nz,)),
             dma((ntp,)),
             dma((ntp,)),
-            dma((ny,)),
-            dma((ny,)),
-            dma((nz,)),
-            dma((nz,)),
-            dma((2,)),
-            dma((2,)),
+            dma((CLASS + 1,)),
+            dma((CLASS + 1,)),
+            dma((CLASS,)),
+            dma((CLASS,)),
+            dma((3,)),
+            dma((3,)),
             dma((nx,)),
             dma((nx,)),
             dma((nx,)),
@@ -557,7 +642,7 @@
         ]
         return pl.pallas_call(
             functools.partial(kernel, sizes),
-            out_shape=jax.ShapeDtypeStruct((TOK, BLOCK), BF16),
+            out_shape=pltpu.VMEM((TOK, BLOCK), BF16),
             in_specs=specs,
             out_specs=pl.BlockSpec(memory_space=pltpu.VMEM),
             scratch_shapes=scratch,

time: 51.5 us -> 46.1 us (0.90)
  Pallas kernels: 49.8 us -> 45.3 us
  local copies, waits for them, and re-layouts: 1.57 us -> 0.66 us
    pallas_call x1, Pallas kernels: 49.8 us -> 45.3 us  [body(): pl.pallas_call(functools.partial(kernel, sizes), out_shape=pltpu.VMEM((TO...]
    unnamed x1, local copies, waits for them, and re-layouts: 1.57 us -> 0.66 us
where the time goes in v2:
time: 46.1 us; the launch traced here: 46 us
  Pallas kernels  45.3 us (98%)
  local copies, waits for them, and re-layouts  0.66 us (1%)
    pallas_call x1, Pallas kernels, body(): pl.pallas_call(functools.partial(kernel, sizes), out_shape=pltpu.VMEM((TO...  45.3 us

profile of v2, /device:TPU:1, one launch (start us, length us, event | category | flops | bytes accessed | tf_op | source)
XLA Modules:
  0.0 46.0 jit_solution(18285728025216016764)
XLA Ops:
  0.0 45.3 %fused_layer.1 = bf16[256,256]{1,0:T(8,128)(2,1)S(1)} custom-call(bf16[256,2048]{1,0:T(8,128)(2,1)} %latent.1, bf16[8,2048]{1,0:T(8,128)(2,1)} %context.1, bf16[1,32]{1,0:T(2,128)(2,1)} %bitcast.8, bf16[1,32]{1,0:T(2,128)(2,1)} %bitcast.9, bf16[32,256]{1,0:T(8,128)(2,1)} %shift_w.1, bf16[32,256]{1,0:T(8,128)(2,1)} %scale_w.1, bf16[32,256]{1,0:T(8,128)(2,1)} %gate_w.1, ...), custom_call_target="tpu_custom_call" | custom-call | tf_op jit(solution)/shard_map/fused_layer/pallas_call | solution.py:643
  45.3 0.7 %copy.17 = bf16[256,256]{1,0:T(8,128)(2,1)} copy(bf16[256,256]{1,0:T(8,128)(2,1)S(1)} %fused_layer.1) | data formatting | bytes 262144
